TPU v7x, 32 devices: a whole 2x2x4 slice. The times are simulated.
32 devices in a mesh: fs: 4 (over z), rep: 4 (over y, x), tp: 2 (over core).
Axes of the slice: x: 2, y: 2, z: 4, core: 2. Of those that a mesh axis runs over, the one named last changes fastest.
Arguments:
- saved_input: bfloat16 [16384, 2048], P(('fs', 'rep')), may hold values from -6 to 6
- cot_input: bfloat16 [16384, 1024], P(('fs', 'rep'), 'tp'), may hold values from -0.046875 to 0.046875
- cot_gate: bfloat16 [16384, 1024], P(('fs', 'rep'), 'tp'), may hold values from -0.046875 to 0.046875
- in_master: float32 [2048, 1024], P('fs', 'tp'), may hold values from -3 to 3
- gate_master: float32 [2048, 1024], P('fs', 'tp'), may hold values from -3 to 3
- in_factor: bfloat16 [2048, 256], P('fs'), may hold values from -0.125 to 0.125
- gate_factor: bfloat16 [2048, 256], P('fs'), may hold values from -0.125 to 0.125
- in_first: float32 [256, 1024], P('fs', 'tp'), may hold values from -6 to 6
- in_second: float32 [256, 1024], P('fs', 'tp'), may hold values from 0.5 to 2
- gate_first: float32 [256, 1024], P('fs', 'tp'), may hold values from -6 to 6
- gate_second: float32 [256, 1024], P('fs', 'tp'), may hold values from 0.5 to 2
Outputs:
- in_master_new: float32 [2048, 1024], P('fs', 'tp')
- gate_master_new: float32 [2048, 1024], P('fs', 'tp')
- in_update: float32 [2048, 1024], P('fs', 'tp')
- gate_update: float32 [2048, 1024], P('fs', 'tp')
- in_first_new: float32 [256, 1024], P('fs', 'tp')
- in_second_new: float32 [256, 1024], P('fs', 'tp')
- gate_first_new: float32 [256, 1024], P('fs', 'tp')
- gate_second_new: float32 [256, 1024], P('fs', 'tp')
- in_copy: bfloat16 [2048, 1024], P(None, 'tp')
- gate_copy: bfloat16 [2048, 1024], P(None, 'tp')
All inputs are finite; a program needn't handle non-finite values.
Results may differ from a plain program's by a relative error of at most 0.0065.
Values may be sent and summed in bfloat16 or wider, within the bound.
No kernel may reach another device: no remote copies, remote signals or barrier semaphores. Data moves between devices by JAX's collectives and lax.ppermute only.
A program may use at most 64 MiB of HBM per device.

v0:
```python
import jax
import jax.numpy as jnp
from jax import lax
from jax.sharding import PartitionSpec as P

D = 2048
W = 1024
CONTRACT_ROWS = (((0,), (0,)), ((), ()))


def plain_rows(left, right):
    return lax.dot_general(left, right, CONTRACT_ROWS, preferred_element_type=jnp.float32)


def split_parts(values):
    upper = values.astype(jnp.bfloat16)
    lower = (values - upper.astype(jnp.float32)).astype(jnp.bfloat16)
    return (upper, lower)


def on_device(
    saved_input,
    cot_input,
    cot_gate,
    in_master,
    gate_master,
    in_factor,
    gate_factor,
    in_first,
    in_second,
    gate_first,
    gate_second,
):
    width = in_master.shape[1]
    in_basis = in_factor.astype(jnp.float32)
    gate_basis = gate_factor.astype(jnp.float32)
    in_whole, gate_whole = (
        lax.all_gather(in_factor, "fs", axis=0, tiled=True),
        lax.all_gather(gate_factor, "fs", axis=0, tiled=True),
    )
    in_upper, in_lower = split_parts(
        jnp.dot(saved_input, in_whole, preferred_element_type=jnp.float32)
    )
    gate_upper, gate_lower = split_parts(
        jnp.dot(saved_input, gate_whole, preferred_element_type=jnp.float32)
    )
    left = plain_rows(in_upper, cot_input)
    left = left + plain_rows(in_lower, cot_input)
    right = plain_rows(gate_upper, cot_gate)
    right = right + plain_rows(gate_lower, cot_gate)
    partial_low = lax.psum_scatter(
        jnp.concatenate([left, right], axis=1).astype(jnp.bfloat16),
        "fs",
        scatter_dimension=0,
        tiled=True,
    )
    low = lax.psum(partial_low, "rep").astype(jnp.float32)
    first_old = jnp.concatenate([in_first, gate_first], axis=1)
    second_old = jnp.concatenate([in_second, gate_second], axis=1)
    first_new = 0.8 * first_old + 0.2 * low
    second_new = 0.95 * second_old + 0.05 * low * low
    normed = first_new / jnp.sqrt(second_new)
    piece = lax.all_gather(normed, "fs", axis=0, tiled=True)
    left = jnp.dot(in_basis, piece[:, :width], precision=lax.Precision.HIGHEST)
    right = jnp.dot(gate_basis, piece[:, width:], precision=lax.Precision.HIGHEST)
    in_square, gate_square = lax.psum((jnp.sum(left * left), jnp.sum(right * right)), ("fs", "tp"))
    in_update = left / jnp.sqrt(in_square / (D * W) + 0.1)
    gate_update = right / jnp.sqrt(gate_square / (D * W) + 0.1)
    in_master_new = in_master - 0.05 * in_update
    gate_master_new = gate_master - 0.05 * gate_update
    in_copy, gate_copy = (
        lax.all_gather(in_master_new.astype(jnp.bfloat16), "fs", axis=0, tiled=True),
        lax.all_gather(gate_master_new.astype(jnp.bfloat16), "fs", axis=0, tiled=True),
    )
    return (
        in_master_new,
        gate_master_new,
        in_update,
        gate_update,
        first_new[:, :width],
        second_new[:, :width],
        first_new[:, width:],
        second_new[:, width:],
        in_copy,
        gate_copy,
    )


def solution(mesh):
    placed = (
        P(("fs", "rep"), None),
        P(("fs", "rep"), "tp"),
        P(("fs", "rep"), "tp"),
        P("fs", "tp"),
        P("fs", "tp"),
        P("fs", None),
        P("fs", None),
        P("fs", "tp"),
        P("fs", "tp"),
        P("fs", "tp"),
        P("fs", "tp"),
    )
    return jax.shard_map(
        on_device,
        mesh=mesh,
        in_specs=placed,
        out_specs=(
            P("fs", "tp"),
            P("fs", "tp"),
            P("fs", "tp"),
            P("fs", "tp"),
            P("fs", "tp"),
            P("fs", "tp"),
            P("fs", "tp"),
            P("fs", "tp"),
            P(None, "tp"),
            P(None, "tp"),
        ),
        check_vma=False,
    )
```

profile of v0, /device:TPU:0, one launch (start us, length us, event | category | flops | bytes accessed | tf_op | source)
XLA Modules:
  0.0 296.7 jit_solution(4529653988439130760)
XLA Ops:
  8.7 31.6 %all-gather.8.cloned.1.call-done = bf16[2048,256]{1,0:T(8,128)(2,1)} async-done(((bf16[512,256]{1,0:T(8,128)(2,1)}), bf16[2048,256]{1,0:T(8,128)(2,1)}) %all-gather.8.cloned.1.call-update) | async-done | bytes 1048592 | tf_op jit(solution)/shard_map/all_gather | solution.py:39
  40.3 3.7 %fusion.21 = f32[1024,256]{1,0:T(8,128)S(1)} fusion(bf16[1024,2048]{1,0:T(8,128)(2,1)} %param.11, bf16[2048,256]{1,0:T(8,128)(2,1)} %all-gather.8.cloned.1.call-done), kind=kOutput, calls=%fused_computation.35 | convolution fusion | flops 1073741824 | bytes 6291456 | tf_op jit(solution)/shard_map/dot_general | solution.py:45
  45.8 23.5 %all-gather.6.cloned.1.call-done = bf16[2048,256]{1,0:T(8,128)(2,1)} async-done(((bf16[512,256]{1,0:T(8,128)(2,1)}), bf16[2048,256]{1,0:T(8,128)(2,1)}) %all-gather.6.cloned.1.call-update) | async-done | bytes 1048592 | tf_op jit(solution)/shard_map/all_gather | solution.py:38
  69.3 3.7 %fusion.20 = f32[1024,256]{1,0:T(8,128)S(1)} fusion(bf16[1024,2048]{1,0:T(8,128)(2,1)} %param.11, bf16[2048,256]{1,0:T(8,128)(2,1)} %all-gather.6.cloned.1.call-done), kind=kOutput, calls=%fused_computation.34 | convolution fusion | flops 1073741824 | bytes 6291456 | tf_op jit(solution)/shard_map/dot_general | solution.py:42
  75.0 21.3 %reduce-scatter.2.cloned.1.call-done = bf16[64,1024]{1,0:T(8,128)(2,1)} async-done(((bf16[256,1024]{1,0:T(8,128)(2,1)}), bf16[64,1024]{1,0:T(8,128)(2,1)}) %reduce-scatter.2.cloned.1.call-update) | async-done | bytes 131088 | tf_op jit(solution)/shard_map/reduce_scatter | solution.py:51
  96.4 43.2 %all-reduce.3.cloned.1.call-done = bf16[64,1024]{1,0:T(8,128)(2,1)} async-done(((bf16[64,1024]{1,0:T(8,128)(2,1)}), bf16[64,1024]{1,0:T(8,128)(2,1)}) %all-reduce.3.cloned.1.call-update) | async-done | bytes 131088 | tf_op jit(solution)/shard_map/psum | solution.py:57
  139.6 2.0 rsqrt_multiply_fusion
  141.7 1.3 copy.21
  143.0 26.8 %all-gather.10.cloned.1.call-done = f32[256,1024]{1,0:T(8,128)} async-done(((f32[64,1024]{1,0:T(8,128)}), f32[256,1024]{1,0:T(8,128)}) %all-gather.10.cloned.1.call-update) | async-done | bytes 1048592 | tf_op jit(solution)/shard_map/all_gather | solution.py:63
  169.8 3.6 %multiply_reduce_fusion = (f32[]{:T(128)}, f32[512,512]{1,0:T(8,128)}) fusion(bf16[512,256]{1,0:T(8,128)(2,1)S(1)} %copy-done.3, f32[256,1024]{1,0:T(8,128)} %all-gather.10.cloned.1.call-done), kind=kOutput, calls=%fused_computation.6 | convolution fusion | flops 805830656 | bytes 1835012 | tf_op jit(solution)/shard_map/dot_general | solution.py:65
  173.4 3.6 %multiply_reduce_fusion.1 = (f32[]{:T(128)}, f32[512,512]{1,0:T(8,128)}) fusion(bf16[512,256]{1,0:T(8,128)(2,1)S(1)} %copy-done.4, f32[256,1024]{1,0:T(8,128)} %all-gather.10.cloned.1.call-done), kind=kOutput, calls=%fused_computation.9 | convolution fusion | flops 805830656 | bytes 1835012 | tf_op jit(solution)/shard_map/dot_general | solution.py:64
  177.0 15.3 %all-reduce = (f32[]{:T(128)}, f32[]{:T(128)}) all-reduce(f32[]{:T(128)} %get-tuple-element.35, f32[]{:T(128)} %get-tuple-element.37), channel_id=1, replica_groups=mesh['fs'=4,'rep'=4,'tp'=2] {'fs','tp'}, use_global_device_ids=true, to_apply=%region_3.0 | all-reduce | flops 2 | bytes 16 | tf_op jit(solution)/shard_map/psum | solution.py:66
  193.0 2.7 fusion.15
  195.7 2.5 copy.22
  199.0 3.4 %fusion.14 = (bf16[512,512]{0,1:T(8,128)(2,1)}, f32[512,512]{0,1:T(8,128)}, f32[512,512]{0,1:T(8,128)}) fusion(f32[512,512]{0,1:T(8,128)} %copy.22, f32[512,512]{1,0:T(8,128)} %get-tuple-element.38, f32[]{:T(128)S(6)} %sqrt.11), kind=kLoop, calls=%fused_computation.30 | loop fusion | flops 1048576 | bytes 4718596 | tf_op jit(solution)/shard_map/convert_element_type | solution.py:73
  202.4 1.8 fusion.18
  204.2 2.5 copy.24
  206.7 2.5 copy.26
  209.3 1.3 copy.23
  210.6 1.3 copy.25
  211.9 28.0 %all-gather.12.cloned.1.call-done = bf16[2048,512]{0,1:T(8,128)(2,1)} async-done(((bf16[512,512]{0,1:T(8,128)(2,1)}), bf16[2048,512]{0,1:T(8,128)(2,1)}) %all-gather.12.cloned.1.call-update) | async-done | bytes 2097168 | tf_op jit(solution)/shard_map/all_gather | solution.py:72
  239.9 3.9 %copy.27 = bf16[2048,512]{1,0:T(8,128)(2,1)} copy(bf16[2048,512]{0,1:T(8,128)(2,1)} %all-gather.12.cloned.1.call-done) | data formatting | bytes 4194304
  243.8 42.1 %all-gather.14.cloned.1.call-done = bf16[2048,512]{0,1:T(8,128)(2,1)} async-done(((bf16[512,512]{0,1:T(8,128)(2,1)}), bf16[2048,512]{0,1:T(8,128)(2,1)}) %all-gather.14.cloned.1.call-update) | async-done | bytes 2097168 | tf_op jit(solution)/shard_map/all_gather | solution.py:73
  285.9 3.9 %copy.28 = bf16[2048,512]{1,0:T(8,128)(2,1)} copy(bf16[2048,512]{0,1:T(8,128)(2,1)} %all-gather.14.cloned.1.call-done) | data formatting | bytes 4194304
  (35 shorter events, 5.3 us)
Async XLA Ops:
  7.2 36.9 %copy-start = (bf16[1024,512]{1,0:T(8,128)(2,1)S(1)}, bf16[1024,512]{1,0:T(8,128)(2,1)}, u32[]{:S(2)}) copy-start(bf16[1024,512]{1,0:T(8,128)(2,1)} %param.13) | copy-start | bytes 3145732
  7.2 33.1 %all-gather.8.cloned.1.call-start = ((), (), s32[]{:S(2)}) async-start(), calls=%async_computation.2 | async-start | bytes 1310720 | tf_op jit(solution)/shard_map/all_gather | solution.py:39
  7.9 61.3 %all-gather.6.cloned.1.call-start = ((), (), s32[]{:S(2)}) async-start(), calls=%async_computation.1 | async-start | bytes 1310720 | tf_op jit(solution)/shard_map/all_gather | solution.py:38
  8.7 87.6 %reduce-scatter.2.cloned.1.call-start = ((), (), s32[]{:S(2)}) async-start(), calls=%async_computation.3 | async-start | bytes 655360 | tf_op jit(solution)/shard_map/reduce_scatter | solution.py:51
  45.8 27.3 %copy-start.1 = (bf16[1024,512]{1,0:T(8,128)(2,1)S(1)}, bf16[1024,512]{1,0:T(8,128)(2,1)}, u32[]{:S(2)}) copy-start(bf16[1024,512]{1,0:T(8,128)(2,1)} %param.12) | copy-start | bytes 3145732
  73.0 1.0 copy-start.6
  73.0 66.5 %copy-start.7 = (f32[64,512]{1,0:T(8,128)S(1)}, f32[64,512]{1,0:T(8,128)}, u32[]{:S(2)}) copy-start(f32[64,512]{1,0:T(8,128)} %param.21) | copy-start | bytes 393220
  73.0 68.6 %copy-start.2 = (f32[512,512]{1,0:T(8,128)S(1)}, f32[512,512]{1,0:T(8,128)}, u32[]{:S(2)}) copy-start(f32[512,512]{1,0:T(8,128)} %param.14) | copy-start | bytes 3145732
  73.5 96.2 %copy-start.3 = (bf16[512,256]{1,0:T(8,128)(2,1)S(1)}, bf16[512,256]{1,0:T(8,128)(2,1)}, u32[]{:S(2)}) copy-start(bf16[512,256]{1,0:T(8,128)(2,1)} %param.17) | copy-start | bytes 786436
  74.1 99.3 %copy-start.4 = (bf16[512,256]{1,0:T(8,128)(2,1)S(1)}, bf16[512,256]{1,0:T(8,128)(2,1)}, u32[]{:S(2)}) copy-start(bf16[512,256]{1,0:T(8,128)(2,1)} %param.16) | copy-start | bytes 786436
  75.0 64.6 %all-reduce.3.cloned.1.call-start = ((), (), s32[]{:S(2)}) async-start(), calls=%async_computation.4 | async-start | bytes 262144 | tf_op jit(solution)/shard_map/psum | solution.py:57
  96.3 73.4 %all-gather.10.cloned.1.call-start = ((), (), s32[]{:S(2)}) async-start(), calls=%async_computation.5 | async-start | bytes 1310720 | tf_op jit(solution)/shard_map/all_gather | solution.py:63
  141.6 98.2 %all-gather.12.cloned.1.call-start = ((), (), s32[]{:S(2)}) async-start(), calls=%async_computation.6 | async-start | bytes 2621440 | tf_op jit(solution)/shard_map/all_gather | solution.py:72
  195.7 6.7 %copy-start.5 = (f32[64,1024]{1,0:T(8,128)S(1)}, f32[64,1024]{1,0:T(8,128)}, u32[]{:S(2)}) copy-start(f32[64,1024]{1,0:T(8,128)} %get-tuple-element.29) | copy-start | bytes 786436
  195.7 90.2 %all-gather.14.cloned.1.call-start = ((), (), s32[]{:S(2)}) async-start(), calls=%async_computation.7 | async-start | bytes 2621440 | tf_op jit(solution)/shard_map/all_gather | solution.py:73
Sparse Core Ops, SparseCore 0:
  9.6 30.6 all-gather.7
  41.9 27.3 all-gather.5
  75.1 21.1 reduce-scatter.1
  99.1 40.4 all-reduce.2
  141.7 27.9 all-gather.9
  195.8 44.0 all-gather.11
  241.4 44.4 all-gather.13
where the time goes:
time: 297 us
  waiting for transfers between devices  218 us (73%)
  local copies, waits for them, and re-layouts  21.2 us (7%)
  matrix products  17.3 us (6%)
  between operations  15.7 us (5%)
  blocking collectives  15.3 us (5%)
  other arithmetic  8.96 us (3%)
    psum x1, waiting for transfers between devices, on_device(): low = lax.psum(partial_low, 'rep').astype(jnp.float32)  43.2 us
    all_gather x1, waiting for transfers between devices, on_device(): lax.all_gather(gate_master_new.astype(jnp.bfloat16), 'fs', axis=0, tiled=...  42.1 us
    all_gather x1, waiting for transfers between devices, on_device(): lax.all_gather(gate_factor, 'fs', axis=0, tiled=True)  31.6 us
    all_gather x1, waiting for transfers between devices, on_device(): lax.all_gather(in_master_new.astype(jnp.bfloat16), 'fs', axis=0, tiled=True)  28 us
    all_gather x1, waiting for transfers between devices, on_device(): piece = lax.all_gather(normed, 'fs', axis=0, tiled=True)  26.8 us
    all_gather x1, waiting for transfers between devices, on_device(): lax.all_gather(in_factor, 'fs', axis=0, tiled=True)  23.5 us
    reduce_scatter x1, waiting for transfers between devices, on_device(): lax.psum_scatter(jnp.concatenate([left, right], axis=1).astype(jnp.bfloat...  21.3 us
    unnamed x24, local copies, waits for them, and re-layouts  19.4 us
  transfers between devices with their start and end apart: 7, of which 7 were waited for; matrix products, arithmetic and copies ran while one was open for 9% of the time, Pallas kernels for 0%

commit v1 on v0

--- a/solution.py
+++ b/solution.py
@@ -1,11 +1,20 @@
+import functools
 import jax
 import jax.numpy as jnp
 from jax import lax
 from jax.sharding import PartitionSpec as P
+from jax.lax import all_gather
 
 D = 2048
 W = 1024
 CONTRACT_ROWS = (((0,), (0,)), ((), ()))
+
+
+def recast_scales(v0, lane_axis):
+    return all_gather(v0, axis_name=lane_axis).sum(axis=0)
+
+
+_draft_pieces_all = functools.partial(recast_scales, lane_axis="rep")
 
 
 def plain_rows(left, right):
@@ -54,7 +63,7 @@
         scatter_dimension=0,
         tiled=True,
     )
-    low = lax.psum(partial_low, "rep").astype(jnp.float32)
+    low = _draft_pieces_all(partial_low).astype(jnp.float32)
     first_old = jnp.concatenate([in_first, gate_first], axis=1)
     second_old = jnp.concatenate([in_second, gate_second], axis=1)
     first_new = 0.8 * first_old + 0.2 * low

time: 297 us -> 262 us (0.88)
  waiting for transfers between devices: 218 us -> 172 us
  blocking collectives: 15.3 us -> 26.3 us
    psum x1 -> x0, waiting for transfers between devices: 43.2 us -> none  [on_device(): low = lax.psum(partial_low, 'rep').astype(jnp.float32)]
    all_gather x0 -> x1, blocking collectives: none -> 11 us  [recast_scales(): return all_gather(v0, axis_name=lane_axis).sum(axis=0)]
  transfers between devices with their start and end apart: 7 -> 6, of which waited for: 7 -> 6; matrix products, arithmetic and copies ran while one was open for 9% -> 10% of each run, Pallas kernels for 0% -> 0%
where the time goes in v1:
time: 262 us
  waiting for transfers between devices  172 us (66%)
  blocking collectives  26.3 us (10%)
  local copies, waits for them, and re-layouts  21.2 us (8%)
  matrix products  17.3 us (7%)
  between operations  15.7 us (6%)
  other arithmetic  8.99 us (3%)
    all_gather x1, waiting for transfers between devices, on_device(): lax.all_gather(gate_master_new.astype(jnp.bfloat16), 'fs', axis=0, tiled=...  42 us
    all_gather x1, waiting for transfers between devices, on_device(): lax.all_gather(gate_factor, 'fs', axis=0, tiled=True)  31.6 us
    all_gather x1, waiting for transfers between devices, on_device(): lax.all_gather(in_master_new.astype(jnp.bfloat16), 'fs', axis=0, tiled=True)  28 us
    all_gather x1, waiting for transfers between devices, on_device(): piece = lax.all_gather(normed, 'fs', axis=0, tiled=True)  24.2 us
    all_gather x1, waiting for transfers between devices, on_device(): lax.all_gather(in_factor, 'fs', axis=0, tiled=True)  23.5 us
    reduce_scatter x1, waiting for transfers between devices, on_device(): lax.psum_scatter(jnp.concatenate([left, right], axis=1).astype(jnp.bfloat...  21.3 us
    unnamed x24, local copies, waits for them, and re-layouts  19.4 us
    psum x1, blocking collectives, on_device(): lax.psum((jnp.sum(left * left), jnp.sum(right * right)), ('fs', 'tp'))  15.3 us
  transfers between devices with their start and end apart: 6, of which 6 were waited for; matrix products, arithmetic and copies ran while one was open for 10% of the time, Pallas kernels for 0%

profile of v1, /device:TPU:0, one launch (start us, length us, event | category | flops | bytes accessed | tf_op | source)
XLA Modules:
  0.0 261.7 jit_solution(11503713809066541637)
XLA Ops:
  8.7 31.6 %all-gather.9.cloned.1.call-done = bf16[2048,256]{1,0:T(8,128)(2,1)} async-done(((bf16[512,256]{1,0:T(8,128)(2,1)}), bf16[2048,256]{1,0:T(8,128)(2,1)}) %all-gather.9.cloned.1.call-update) | async-done | bytes 1048592 | tf_op jit(solution)/shard_map/all_gather | solution.py:48
  40.3 3.7 %fusion.21 = f32[1024,256]{1,0:T(8,128)S(1)} fusion(bf16[1024,2048]{1,0:T(8,128)(2,1)} %param.11, bf16[2048,256]{1,0:T(8,128)(2,1)} %all-gather.9.cloned.1.call-done), kind=kOutput, calls=%fused_computation.35 | convolution fusion | flops 1073741824 | bytes 6291456 | tf_op jit(solution)/shard_map/dot_general | solution.py:54
  45.8 23.5 %all-gather.7.cloned.1.call-done = bf16[2048,256]{1,0:T(8,128)(2,1)} async-done(((bf16[512,256]{1,0:T(8,128)(2,1)}), bf16[2048,256]{1,0:T(8,128)(2,1)}) %all-gather.7.cloned.1.call-update) | async-done | bytes 1048592 | tf_op jit(solution)/shard_map/all_gather | solution.py:47
  69.3 3.7 %fusion.20 = f32[1024,256]{1,0:T(8,128)S(1)} fusion(bf16[1024,2048]{1,0:T(8,128)(2,1)} %param.11, bf16[2048,256]{1,0:T(8,128)(2,1)} %all-gather.7.cloned.1.call-done), kind=kOutput, calls=%fused_computation.34 | convolution fusion | flops 1073741824 | bytes 6291456 | tf_op jit(solution)/shard_map/dot_general | solution.py:51
  75.0 21.3 %reduce-scatter.2.cloned.1.call-done = bf16[64,1024]{1,0:T(8,128)(2,1)} async-done(((bf16[256,1024]{1,0:T(8,128)(2,1)}), bf16[64,1024]{1,0:T(8,128)(2,1)}) %reduce-scatter.2.cloned.1.call-update) | async-done | bytes 131088 | tf_op jit(solution)/shard_map/reduce_scatter | solution.py:60
  96.4 11.0 %all-gather = bf16[256,1024]{1,0:T(8,128)(2,1)S(1)} all-gather(bf16[64,1024]{1,0:T(8,128)(2,1)} %reduce-scatter.2.cloned.1.call-done), channel_id=2, replica_groups=mesh['fs'=4,'rep'=4,'tp'=2] {'rep'}, dimensions={0}, use_global_device_ids=true | all-gather | bytes 655360 | tf_op jit(solution)/shard_map/all_gather | solution.py:14
  107.4 2.0 rsqrt_multiply_fusion
  109.5 1.3 copy.21
  110.8 24.2 %all-gather.11.cloned.1.call-done = f32[256,1024]{1,0:T(8,128)} async-done(((f32[64,1024]{1,0:T(8,128)}), f32[256,1024]{1,0:T(8,128)}) %all-gather.11.cloned.1.call-update) | async-done | bytes 1048592 | tf_op jit(solution)/shard_map/all_gather | solution.py:72
  134.9 3.6 %multiply_reduce_fusion = (f32[]{:T(128)}, f32[512,512]{1,0:T(8,128)}) fusion(bf16[512,256]{1,0:T(8,128)(2,1)S(1)} %copy-done.3, f32[256,1024]{1,0:T(8,128)} %all-gather.11.cloned.1.call-done), kind=kOutput, calls=%fused_computation.6 | convolution fusion | flops 805830656 | bytes 1835012 | tf_op jit(solution)/shard_map/dot_general | solution.py:74
  138.6 3.6 %multiply_reduce_fusion.1 = (f32[]{:T(128)}, f32[512,512]{1,0:T(8,128)}) fusion(bf16[512,256]{1,0:T(8,128)(2,1)S(1)} %copy-done.4, f32[256,1024]{1,0:T(8,128)} %all-gather.11.cloned.1.call-done), kind=kOutput, calls=%fused_computation.9 | convolution fusion | flops 805830656 | bytes 1835012 | tf_op jit(solution)/shard_map/dot_general | solution.py:73
  142.2 15.3 %all-reduce = (f32[]{:T(128)}, f32[]{:T(128)}) all-reduce(f32[]{:T(128)} %get-tuple-element.35, f32[]{:T(128)} %get-tuple-element.37), channel_id=1, replica_groups=mesh['fs'=4,'rep'=4,'tp'=2] {'fs','tp'}, use_global_device_ids=true, to_apply=%region_3.0 | all-reduce | flops 2 | bytes 16 | tf_op jit(solution)/shard_map/psum | solution.py:75
  158.2 2.7 %fusion.15 = (bf16[512,512]{0,1:T(8,128)(2,1)}, f32[512,512]{0,1:T(8,128)S(1)}, f32[512,512]{0,1:T(8,128)S(1)}) fusion(f32[512,512]{0,1:T(8,128)} %copy.21, f32[512,512]{1,0:T(8,128)} %get-tuple-element.36, f32[]{:T(128)S(6)} %sqrt.10), kind=kLoop, calls=%fused_computation.31 | loop fusion | flops 1048576 | bytes 4718596 | tf_op jit(solution)/shard_map/convert_element_type | solution.py:81
  160.9 2.5 copy.22
  164.1 3.4 %fusion.14 = (bf16[512,512]{0,1:T(8,128)(2,1)}, f32[512,512]{0,1:T(8,128)}, f32[512,512]{0,1:T(8,128)}) fusion(f32[512,512]{0,1:T(8,128)} %copy.22, f32[512,512]{1,0:T(8,128)} %get-tuple-element.38, f32[]{:T(128)S(6)} %sqrt.11), kind=kLoop, calls=%fused_computation.30 | loop fusion | flops 1048576 | bytes 4718596 | tf_op jit(solution)/shard_map/convert_element_type | solution.py:82
  167.6 1.8 fusion.18
  169.4 2.5 copy.24
  171.9 2.5 copy.26
  174.4 1.3 copy.23
  175.7 1.3 copy.25
  177.1 28.0 %all-gather.13.cloned.1.call-done = bf16[2048,512]{0,1:T(8,128)(2,1)} async-done(((bf16[512,512]{0,1:T(8,128)(2,1)}), bf16[2048,512]{0,1:T(8,128)(2,1)}) %all-gather.13.cloned.1.call-update) | async-done | bytes 2097168 | tf_op jit(solution)/shard_map/all_gather | solution.py:81
  205.0 3.9 %copy.27 = bf16[2048,512]{1,0:T(8,128)(2,1)} copy(bf16[2048,512]{0,1:T(8,128)(2,1)} %all-gather.13.cloned.1.call-done) | data formatting | bytes 4194304
  208.9 42.0 %all-gather.15.cloned.1.call-done = bf16[2048,512]{0,1:T(8,128)(2,1)} async-done(((bf16[512,512]{0,1:T(8,128)(2,1)}), bf16[2048,512]{0,1:T(8,128)(2,1)}) %all-gather.15.cloned.1.call-update) | async-done | bytes 2097168 | tf_op jit(solution)/shard_map/all_gather | solution.py:82
  251.0 3.9 %copy.28 = bf16[2048,512]{1,0:T(8,128)(2,1)} copy(bf16[2048,512]{0,1:T(8,128)(2,1)} %all-gather.15.cloned.1.call-done) | data formatting | bytes 4194304
  (34 shorter events, 5.3 us)
Async XLA Ops:
  7.2 36.9 %copy-start = (bf16[1024,512]{1,0:T(8,128)(2,1)S(1)}, bf16[1024,512]{1,0:T(8,128)(2,1)}, u32[]{:S(2)}) copy-start(bf16[1024,512]{1,0:T(8,128)(2,1)} %param.13) | copy-start | bytes 3145732
  7.2 33.1 %all-gather.9.cloned.1.call-start = ((), (), s32[]{:S(2)}) async-start(), calls=%async_computation.2 | async-start | bytes 1310720 | tf_op jit(solution)/shard_map/all_gather | solution.py:48
  7.9 61.3 %all-gather.7.cloned.1.call-start = ((), (), s32[]{:S(2)}) async-start(), calls=%async_computation.1 | async-start | bytes 1310720 | tf_op jit(solution)/shard_map/all_gather | solution.py:47
  8.7 87.7 %reduce-scatter.2.cloned.1.call-start = ((), (), s32[]{:S(2)}) async-start(), calls=%async_computation.3 | async-start | bytes 655360 | tf_op jit(solution)/shard_map/reduce_scatter | solution.py:60
  45.8 27.3 %copy-start.1 = (bf16[1024,512]{1,0:T(8,128)(2,1)S(1)}, bf16[1024,512]{1,0:T(8,128)(2,1)}, u32[]{:S(2)}) copy-start(bf16[1024,512]{1,0:T(8,128)(2,1)} %param.12) | copy-start | bytes 3145732
  73.0 1.0 copy-start.6
  73.0 34.4 %copy-start.7 = (f32[64,512]{1,0:T(8,128)S(1)}, f32[64,512]{1,0:T(8,128)}, u32[]{:S(2)}) copy-start(f32[64,512]{1,0:T(8,128)} %param.21) | copy-start | bytes 393220
  73.5 35.9 %copy-start.2 = (f32[512,512]{1,0:T(8,128)S(1)}, f32[512,512]{1,0:T(8,128)}, u32[]{:S(2)}) copy-start(f32[512,512]{1,0:T(8,128)} %param.14) | copy-start | bytes 3145732
  73.5 61.4 %copy-start.3 = (bf16[512,256]{1,0:T(8,128)(2,1)S(1)}, bf16[512,256]{1,0:T(8,128)(2,1)}, u32[]{:S(2)}) copy-start(bf16[512,256]{1,0:T(8,128)(2,1)} %param.17) | copy-start | bytes 786436
  74.1 64.5 %copy-start.4 = (bf16[512,256]{1,0:T(8,128)(2,1)S(1)}, bf16[512,256]{1,0:T(8,128)(2,1)}, u32[]{:S(2)}) copy-start(bf16[512,256]{1,0:T(8,128)(2,1)} %param.16) | copy-start | bytes 786436
  75.0 60.0 %all-gather.11.cloned.1.call-start = ((), (), s32[]{:S(2)}) async-start(), calls=%async_computation.4 | async-start | bytes 1310720 | tf_op jit(solution)/shard_map/all_gather | solution.py:72
  109.4 95.6 %all-gather.13.cloned.1.call-start = ((), (), s32[]{:S(2)}) async-start(), calls=%async_computation.5 | async-start | bytes 2621440 | tf_op jit(solution)/shard_map/all_gather | solution.py:81
  160.8 6.7 %copy-start.5 = (f32[64,1024]{1,0:T(8,128)S(1)}, f32[64,1024]{1,0:T(8,128)}, u32[]{:S(2)}) copy-start(f32[64,1024]{1,0:T(8,128)} %get-tuple-element.29) | copy-start | bytes 786436
  160.9 90.1 %all-gather.15.cloned.1.call-start = ((), (), s32[]{:S(2)}) async-start(), calls=%async_computation.6 | async-start | bytes 2621440 | tf_op jit(solution)/shard_map/all_gather | solution.py:82
Sparse Core Ops, SparseCore 0:
  9.6 30.6 all-gather.8
  41.9 27.3 all-gather.6
  75.1 21.2 reduce-scatter.1
  109.5 25.3 all-gather.10
  161.0 44.0 all-gather.12
  206.5 44.4 all-gather.14
